TPU v7x, 32 devices: a whole 2x2x4 slice. The times are simulated.
32 devices in a mesh: grp: 2 (over y), st: 4 (over z), tp: 4 (over x, core).
Axes of the slice: x: 2, y: 2, z: 4, core: 2. Of those that a mesh axis runs over, the one named last changes fastest.
Arguments:
- tokens: bfloat16 [4096, 2048], P(('grp', 'st'), 'tp'), parts along dimension 0, may hold values from -180 to 180
- ret_query: bfloat16 [4096, 1024], P(('grp', 'st'), 'tp'), parts along dimension 0, may hold values from -6 to 6
- ret_key: bfloat16 [4096, 1024], P(('grp', 'st'), 'tp'), parts along dimension 0, may hold values from -6 to 6
- ret_value: bfloat16 [4096, 1024], P(('grp', 'st'), 'tp'), parts along dimension 0, may hold values from -6 to 6
- w_query: bfloat16 [2048, 2048], P(None, 'tp'), may hold values from -0.125 to 0.125
- w_key: bfloat16 [2048, 2048], P(None, 'tp'), may hold values from -0.125 to 0.125
- w_value: bfloat16 [2048, 2048], P(None, 'tp'), may hold values from -0.125 to 0.125
- w_gate: bfloat16 [2048, 4], replicated, may hold values from -0.125 to 0.125
- store: bfloat16 [24, 128, 2048], P('st'), may hold values from -6 to 6
- passage_ids: int32 [64, 4], P(('grp', 'st')), parts along dimension 0, may hold values from 0 to 23, as said below
Outputs:
- blended: bfloat16 [4096, 3072], P(('grp', 'st'), 'tp'), parts along dimension 0
There are 2 independent parts, one for each index of `grp`. A program takes and returns all parts, laid end to end along the dimension named above; an argument that names none is the same for every part. Nothing has to cross between parts.
Inputs may be any that keep to these rules, and one draw needn't show every extreme that they name: `passage_ids`: passage p lies on index p // 6 of st. The 8 rows of one device name passages of any one index of st at most 16 times in all, and those of some index exactly 16 times.
All inputs are finite; a program needn't handle non-finite values.
Results may differ from a plain program's by a relative error of at most 0.0094.
Values may be sent and summed in bfloat16 or wider, within the bound.
A program may use at most 128 MiB of HBM per device.

v0:
```python
import jax
import jax.numpy as jnp
from jax import lax
from jax.sharding import PartitionSpec as P

RET_DIM = 256
HEAD_DIM = 512
BLOCK = 64
NPB = 4
SEQ_LEN = 256


ROTARY_BASE = 10000.0
NORM_EPS = 1e-05


def rotate(values, positions):
    halfway = values.shape[-1] // 2
    inverse = ROTARY_BASE ** (-jnp.arange(halfway, dtype=jnp.float32) / halfway)
    angles = positions.astype(jnp.float32)[:, None, None] * inverse
    cosines, sines = (jnp.cos(angles), jnp.sin(angles))
    leading, trailing = (values[..., :halfway], values[..., halfway:])
    return jnp.concatenate(
        [leading * cosines - trailing * sines, leading * sines + trailing * cosines], axis=-1
    )


def retain(query_rows, key_rows, value_rows, head_start):
    token_count = query_rows.shape[0]
    groups = query_rows.shape[1] // RET_DIM
    layout = (token_count // SEQ_LEN, SEQ_LEN, groups, RET_DIM)
    places = jnp.arange(SEQ_LEN, dtype=jnp.int32)
    rot_query = rotate(query_rows.reshape(layout).astype(jnp.float32), places).astype(jnp.bfloat16)
    rot_key = (
        rotate(key_rows.reshape(layout).astype(jnp.float32), places) * RET_DIM ** (-0.5)
    ).astype(jnp.bfloat16)
    head_number = (head_start + jnp.arange(groups, dtype=jnp.int32)).astype(jnp.float32)
    log_gamma = jnp.log1p(-jnp.exp2(-5.0 - head_number))
    offsets = (places[:, None] - places[None, :]).astype(jnp.float32)
    decays = jnp.where(
        offsets[None] >= 0.0,
        jnp.exp(log_gamma[:, None, None] * jnp.maximum(offsets, 0.0)[None]),
        0.0,
    )
    scores = jnp.einsum("sigd,sjgd->sgij", rot_query, rot_key, preferred_element_type=jnp.float32)
    weights = (scores * decays[None]).astype(jnp.bfloat16)
    output = jnp.einsum(
        "sgij,sjge->sige", weights, value_rows.reshape(layout), preferred_element_type=jnp.float32
    )
    centred = output - jnp.mean(output, -1, keepdims=True)
    normed = centred * lax.rsqrt(jnp.mean(centred * centred, -1, keepdims=True) + NORM_EPS)
    return normed.astype(jnp.bfloat16).reshape(token_count, groups, RET_DIM)


def partial_attend(query_block, kv_rows, head_width):
    leading = kv_rows.shape[:-2]
    groups = query_block.shape[-2]
    split_shape = leading + (kv_rows.shape[-2], groups, HEAD_DIM)
    key_part = kv_rows[..., :head_width].reshape(split_shape)
    value_part = kv_rows[..., head_width:].reshape(split_shape)
    scores = jnp.einsum(
        "...tgd,...rgd->...gtr", query_block, key_part, preferred_element_type=jnp.float32
    ) * HEAD_DIM ** (-0.5)
    highest = jnp.max(scores, -1)
    exponent = jnp.exp(scores - highest[..., None])
    totals = jnp.sum(exponent, -1)
    weighted = jnp.einsum(
        "...gtr,...rgd->...tgd",
        exponent.astype(jnp.bfloat16),
        value_part,
        preferred_element_type=jnp.float32,
    )
    return (
        weighted.astype(jnp.bfloat16).reshape(leading + (query_block.shape[-3], head_width)),
        highest,
        totals,
    )


def combine(weighted, highest, totals, gate_vals):
    block_count, per_block, span_len, head_width = weighted.shape
    groups = highest.shape[2]
    overall = jnp.max(highest, 1, keepdims=True)
    scales = jnp.exp(highest - overall)
    denominator = jnp.sum(scales * totals, 1)
    pieces = (
        lax.optimization_barrier(weighted)
        .reshape(block_count, per_block, span_len, groups, head_width // groups)
        .astype(jnp.float32)
    )
    numerator = jnp.sum(jnp.transpose(scales, (0, 1, 3, 2))[..., None] * pieces, 1)
    gate_cols = gate_vals.reshape(block_count, span_len, groups)[..., None]
    result = gate_cols * numerator / jnp.transpose(denominator, (0, 2, 1))[..., None]
    return result.astype(jnp.bfloat16).reshape(block_count * span_len, groups, head_width // groups)


def body(
    tokens, ret_query, ret_key, ret_value, w_query, w_key, w_value, w_gate, store, passage_ids
):
    owners = lax.axis_size("st")
    head_rank = lax.axis_index("tp")
    groups = w_query.shape[1] // HEAD_DIM
    head_width = groups * HEAD_DIM
    token_count = tokens.shape[0]
    block_count = token_count // BLOCK
    retained = retain(ret_query, ret_key, ret_value, head_rank * groups)
    shard_cols = lax.all_gather(tokens, "tp", axis=1, tiled=True)
    query_sum = jnp.dot(shard_cols, w_query, preferred_element_type=jnp.float32)
    gate_sum = jnp.dot(shard_cols, w_gate, preferred_element_type=jnp.float32)
    gate_vals = jax.nn.sigmoid(lax.dynamic_slice_in_dim(gate_sum, head_rank * groups, groups, 1))
    query_blocks = query_sum.astype(jnp.bfloat16).reshape(block_count, BLOCK, groups, HEAD_DIM)
    kv_own = jnp.concatenate(
        [
            jnp.dot(store, w_key, preferred_element_type=jnp.float32).astype(jnp.bfloat16),
            jnp.dot(store, w_value, preferred_element_type=jnp.float32).astype(jnp.bfloat16),
        ],
        axis=-1,
    )
    flat_ids = passage_ids.reshape(-1)
    requests = flat_ids.shape[0]
    capacity = max(2, 2 * requests // owners)
    owner_of = flat_ids // store.shape[0]
    within = flat_ids % store.shape[0]
    hit_table = (owner_of[:, None] == jnp.arange(owners, dtype=jnp.int32)[None, :]).astype(
        jnp.int32
    )
    earlier = (
        jnp.arange(requests, dtype=jnp.int32)[:, None]
        > jnp.arange(requests, dtype=jnp.int32)[None, :]
    ).astype(jnp.int32)
    slot_of = jnp.sum(jnp.dot(earlier, hit_table) * hit_table, 1)
    placed = (
        hit_table[:, :, None]
        * (slot_of[:, None] == jnp.arange(capacity, dtype=jnp.int32)[None, :]).astype(jnp.int32)[
            :, None, :
        ]
    )
    wanted = jnp.sum(placed * within[:, None, None], 0)
    fetch_at = owner_of * capacity + slot_of
    block_of = jnp.sum(placed * (jnp.arange(requests, dtype=jnp.int32) // NPB)[:, None, None], 0)
    outgoing = jnp.take(query_blocks, block_of, axis=0)
    incoming = lax.all_to_all(outgoing, "st", split_axis=0, concat_axis=0, tiled=True)
    indices = lax.all_to_all(wanted, "st", split_axis=0, concat_axis=0, tiled=True)
    weighted_here, highest_here, totals_here = partial_attend(
        incoming, jnp.take(kv_own, indices, axis=0), head_width
    )
    back_values = lax.all_to_all(weighted_here, "st", split_axis=0, concat_axis=0, tiled=True)
    returned = (
        back_values,
        lax.all_to_all(highest_here, "st", split_axis=0, concat_axis=0, tiled=True),
        lax.all_to_all(totals_here, "st", split_axis=0, concat_axis=0, tiled=True),
    )
    weighted = jnp.take(
        returned[0].reshape((owners * capacity,) + returned[0].shape[2:]), fetch_at, axis=0
    )
    weighted = weighted.reshape(block_count, NPB, BLOCK, head_width)
    highest = jnp.take(
        returned[1].reshape((owners * capacity,) + returned[1].shape[2:]), fetch_at, axis=0
    )
    highest = highest.reshape(block_count, NPB, groups, BLOCK)
    totals = jnp.take(
        returned[2].reshape((owners * capacity,) + returned[2].shape[2:]), fetch_at, axis=0
    )
    totals = totals.reshape(block_count, NPB, groups, BLOCK)
    retrieved = combine(weighted, highest, totals, gate_vals)
    return jnp.concatenate([retained, retrieved], -1).reshape(
        token_count, groups * (RET_DIM + HEAD_DIM)
    )


def solution(mesh):
    placed = (
        P(("grp", "st"), "tp"),
        P(("grp", "st"), "tp"),
        P(("grp", "st"), "tp"),
        P(("grp", "st"), "tp"),
        P(None, "tp"),
        P(None, "tp"),
        P(None, "tp"),
        P(),
        P("st", None, None),
        P(("grp", "st"), None),
    )
    return jax.shard_map(
        body, mesh=mesh, in_specs=placed, out_specs=P(("grp", "st"), "tp"), check_vma=False
    )
```

profile of v0, /device:TPU:0, one launch (start us, length us, event | category | flops | bytes accessed | tf_op | source)
XLA Modules:
  0.0 282.8 jit_solution(17544090922661413321)
XLA Ops:
  6.5 0.7 all-gather.2.cloned.1.call-update
  7.3 1.0 copy.24
  8.2 0.1 div.85
  8.3 0.1 rem.43
  8.4 0.1 ne.87
  8.5 0.1 fusion.20
  8.7 0.8 fusion.40
  9.5 6.3 %all-to-all-start.1 = ((s32[4,1,16]{2,1,0:T(1,128)}), s32[4,1,16]{2,1,0:T(1,128)S(1)}, u32[]{:S(2)}, u32[]{:S(2)}) async-start(s32[4,1,16]{2,1,0:T(1,128)} %bitcast.21), calls=%async_computation.1 | async-start | bytes 4096 | tf_op jit(solution)/shard_map/all_to_all | solution.py:143
  15.8 0.1 reshape.675
  15.9 18.3 %all-gather.2.cloned.1.call-done = bf16[512,2048]{1,0:T(8,128)(2,1)} async-done(((bf16[512,512]{1,0:T(8,128)(2,1)}), bf16[512,2048]{1,0:T(8,128)(2,1)}) %all-gather.2.cloned.1.call-update) | async-done | bytes 2097168 | tf_op jit(solution)/shard_map/all_gather | solution.py:107
  34.2 4.3 %convolution_convert_fusion = bf16[512,512]{1,0:T(8,128)(2,1)} fusion(bf16[512,2048]{1,0:T(8,128)(2,1)} %all-gather.2.cloned.1.call-done, bf16[2048,512]{1,0:T(8,128)(2,1)} %param.16), kind=kOutput, calls=%fused_computation.26 | convolution fusion | flops 1074003968 | bytes 4718592 | tf_op jit(solution)/shard_map/dot_general | solution.py:108
  38.5 3.8 %gather_fusion = bf16[64,64,512]{2,1,0:T(8,128)(2,1)} fusion(bf16[8,64,512]{2,1,0:T(8,128)(2,1)} %bitcast.103, s32[1024]{0:T(1024)S(1)} %pad_clamp_fusion.3), kind=kCustom, calls=%fused_computation.2 | custom fusion | bytes 8388864 | tf_op jit(solution)/shard_map/jit(_take)/gather | solution.py:141
  42.3 4.7 %broadcast_select_fusion.1 = bf16[4,16,64,1,512]{4,2,1,3,0:T(8,128)(2,1)} fusion(bf16[4,16,64,1,512]{4,2,1,3,0:T(8,128)(2,1)} %bitcast.104, pred[4,16]{1,0:T(4,128)(4,1)S(1)} %compare_and_fusion.4), kind=kLoop, calls=%fused_computation.13 | loop fusion | flops 2097152 | bytes 8388672 | tf_op jit(solution)/shard_map/jit(_take)/select_n | solution.py:141
  46.9 4.8 %all-to-all-start = ((bf16[4,16,64,1,512]{4,2,1,3,0:T(8,128)(2,1)}), bf16[4,16,64,1,512]{4,2,1,3,0:T(8,128)(2,1)}, u32[]{:S(2)}, u32[]{:S(2)}) async-start(bf16[4,16,64,1,512]{4,2,1,3,0:T(8,128)(2,1)} %broadcast_select_fusion.1), calls=%async_computation | async-start | bytes 8388608 | tf_op jit(solution)/shard_map/all_to_all | solution.py:142
  51.8 0.0 copy-start.9
  51.8 3.5 %fusion.13 = bf16[6,128,512]{2,1,0:T(8,128)(2,1)S(1)} fusion(bf16[6,128,2048]{2,1,0:T(8,128)(2,1)S(1)} %copy-done, bf16[2048,512]{1,0:T(8,128)(2,1)} %param.17), kind=kOutput, calls=%fused_computation.24 | convolution fusion | flops 1611005952 | bytes 6029312 | tf_op jit(solution)/shard_map/dot_general | solution.py:114
  55.3 1.8 fusion.16
  57.1 0.2 pad_maximum_fusion
  57.4 0.1 reshape.683
  57.4 7.5 %gather_fusion.1 = bf16[64,128,1024]{2,1,0:T(8,128)(2,1)} fusion(bf16[6,128,1024]{2,1,0:T(8,128)(2,1)S(1)} %pad_maximum_fusion, s32[1024]{0:T(1024)S(1)} %pad_clamp_fusion.2), kind=kCustom, calls=%fused_computation.3 | custom fusion | bytes 33554688 | tf_op jit(solution)/shard_map/jit(_take)/gather | solution.py:145
  65.0 14.2 %broadcast_select_fusion = bf16[4,16,128,1024]{3,2,1,0:T(8,128)(2,1)} fusion(bf16[4,16,128,1024]{3,2,1,0:T(8,128)(2,1)} %bitcast.102, pred[4,16]{1,0:T(4,128)(4,1)S(1)} %compare_and_fusion.3), kind=kLoop, calls=%fused_computation.5 | loop fusion | flops 8388608 | bytes 33554496 | tf_op jit(solution)/shard_map/jit(_take)/select_n | solution.py:145
  79.2 66.4 %all-to-all-done = bf16[4,16,64,1,512]{4,2,1,3,0:T(8,128)(2,1)} async-done(((bf16[4,16,64,1,512]{4,2,1,3,0:T(8,128)(2,1)}), bf16[4,16,64,1,512]{4,2,1,3,0:T(8,128)(2,1)}, u32[]{:S(2)}, u32[]{:S(2)}) %all-to-all-start) | async-done | bytes 4194336 | tf_op jit(solution)/shard_map/all_to_all | solution.py:142
  145.6 7.7 %multiply_reduce_fusion.1 = (f32[4,16,64]{2,1,0:T(8,128)S(1)}, f32[4,16,64,128]{3,2,1,0:T(8,128)S(1)}) fusion(bf16[4,16,128,1024]{3,2,1,0:T(8,128)(2,1)} %broadcast_select_fusion, bf16[4,16,64,1,512]{4,2,1,3,0:T(8,128)(2,1)} %all-to-all-done), kind=kOutput, calls=%fused_computation.20 | convolution fusion | flops 537915392 | bytes 14696448 | tf_op jit(solution)/shard_map/...tgd,...rgd->...gtr/dot_general | solution.py:61
  153.3 1.3 fusion.11
  154.7 0.7 reshape.715
  155.4 3.3 %all-to-all-start.4 = ((f32[4,1,1024]{2,1,0:T(1,128)}), f32[4,1,1024]{2,1,0:T(1,128)S(1)}, u32[]{:S(2)}, u32[]{:S(2)}) async-start(f32[4,1,1024]{2,1,0:T(1,128)} %reshape.715), calls=%async_computation.4 | async-start | bytes 32768 | tf_op jit(solution)/shard_map/all_to_all | solution.py:151
  158.6 0.7 reshape.713
  159.3 4.9 %all-to-all-done.4 = f32[4,1,1024]{2,1,0:T(1,128)S(1)} async-done(((f32[4,1,1024]{2,1,0:T(1,128)}), f32[4,1,1024]{2,1,0:T(1,128)S(1)}, u32[]{:S(2)}, u32[]{:S(2)}) %all-to-all-start.4) | async-done | bytes 16416 | tf_op jit(solution)/shard_map/all_to_all | solution.py:151
  164.2 3.2 %all-to-all-start.2 = ((f32[4,1,1024]{2,1,0:T(1,128)}), f32[4,1,1024]{2,1,0:T(1,128)S(1)}, u32[]{:S(2)}, u32[]{:S(2)}) async-start(f32[4,1,1024]{2,1,0:T(1,128)} %reshape.713), calls=%async_computation.2 | async-start | bytes 32768 | tf_op jit(solution)/shard_map/all_to_all | solution.py:150
  167.5 5.6 %convert_bitcast_fusion = bf16[4,16,64,512]{3,2,1,0:T(8,128)(2,1)} fusion(bf16[4,16,128,1024]{3,2,1,0:T(8,128)(2,1)} %broadcast_select_fusion, f32[4,16,64,128]{3,2,1,0:T(8,128)S(1)} %get-tuple-element.27, f32[4,16,64]{2,1,0:T(8,128)S(1)} %get-tuple-element.26), kind=kOutput, calls=%fused_computation.12 | convolution fusion | flops 540540928 | bytes 14696448 | tf_op jit(solution)/shard_map/...gtr,...rgd->...tgd/dot_general | solution.py:67
  173.0 0.0 all-to-all-done.2
  173.0 0.6 copy-done.5
  173.6 5.0 %all-to-all-start.3 = ((bf16[4,16,64,512]{3,2,1,0:T(8,128)(2,1)}), bf16[4,16,64,512]{3,2,1,0:T(8,128)(2,1)}, u32[]{:S(2)}, u32[]{:S(2)}) async-start(bf16[4,16,64,512]{3,2,1,0:T(8,128)(2,1)} %convert_bitcast_fusion), calls=%async_computation.3 | async-start | bytes 8388608 | tf_op jit(solution)/shard_map/all_to_all | solution.py:147
  178.7 0.1 reduce_sum.88
  178.8 0.1 div.88
  178.8 0.6 compare_and_fusion
  179.4 0.1 and.76
  179.7 0.6 compare_and_fusion.2
  180.3 0.6 pad_clamp_fusion.1
  180.9 0.6 pad_clamp_fusion
  181.5 0.1 exponential_select_fusion
  181.6 0.5 multiply_cosine_fusion
  182.2 0.8 fusion.38
  182.9 2.3 fusion.57
  185.2 0.7 broadcast_multiply_fusion
  185.9 0.2 multiply_reduce_fusion.2
  186.2 0.2 multiply_convert_fusion
  186.4 1.4 fusion.62
  187.8 0.5 broadcast.484
  188.3 0.7 reduce.10
  189.0 0.1 reshape.716
  189.1 0.7 reduce.11
  189.8 0.1 reshape.714
  189.9 0.7 gather_fusion.4
  190.6 0.7 gather_fusion.3
  191.3 0.1 bitcast_select_fusion
  191.4 0.1 div.89
  191.5 79.0 %all-to-all-done.3 = bf16[4,16,64,512]{3,2,1,0:T(8,128)(2,1)} async-done(((bf16[4,16,64,512]{3,2,1,0:T(8,128)(2,1)}), bf16[4,16,64,512]{3,2,1,0:T(8,128)(2,1)}, u32[]{:S(2)}, u32[]{:S(2)}) %all-to-all-start.3) | async-done | bytes 4194336 | tf_op jit(solution)/shard_map/all_to_all | solution.py:147
  270.5 3.0 %gather_fusion.2 = bf16[32,64,512]{2,1,0:T(8,128)(2,1)S(1)} fusion(bf16[64,64,512]{2,1,0:T(8,128)(2,1)} %bitcast.35, s32[1024]{0:T(1024)} %pad_clamp_fusion), kind=kCustom, calls=%fused_computation.4 | custom fusion | bytes 4194432 | tf_op jit(solution)/shard_map/jit(_take)/gather | solution.py:153
  273.5 0.3 broadcast_select_fusion.2
  273.8 0.5 multiply_reduce_fusion
  274.3 0.2 fusion.23
  274.5 0.9 maximum_bitcast_fusion
  275.4 0.5 copy-done.1
  (42 shorter events, 0.3 us)
Async XLA Ops:
  6.5 45.2 %copy-start = (bf16[6,128,2048]{2,1,0:T(8,128)(2,1)S(1)}, bf16[6,128,2048]{2,1,0:T(8,128)(2,1)}, u32[]{:S(2)}) copy-start(bf16[6,128,2048]{2,1,0:T(8,128)(2,1)} %param.20) | copy-start | bytes 9437188
  6.5 27.7 %all-gather.2.cloned.1.call-start = ((), (), s32[]{:S(2)}) async-start(), calls=%async_computation.5 | async-start | bytes 2621440 | tf_op jit(solution)/shard_map/all_gather | solution.py:107
  9.5 37.5 %all-to-all-start.1 = ((s32[4,1,16]{2,1,0:T(1,128)}), s32[4,1,16]{2,1,0:T(1,128)S(1)}, u32[]{:S(2)}, u32[]{:S(2)}) async-start(s32[4,1,16]{2,1,0:T(1,128)} %bitcast.21), calls=%async_computation.1 | async-start | bytes 4096 | tf_op jit(solution)/shard_map/all_to_all | solution.py:143
  46.9 98.7 %all-to-all-start = ((bf16[4,16,64,1,512]{4,2,1,3,0:T(8,128)(2,1)}), bf16[4,16,64,1,512]{4,2,1,3,0:T(8,128)(2,1)}, u32[]{:S(2)}, u32[]{:S(2)}) async-start(bf16[4,16,64,1,512]{4,2,1,3,0:T(8,128)(2,1)} %broadcast_select_fusion.1), calls=%async_computation | async-start | bytes 8388608 | tf_op jit(solution)/shard_map/all_to_all | solution.py:142
  51.8 3.5 %copy-start.9 = (bf16[2048,512]{1,0:T(8,128)(2,1)S(1)}, bf16[2048,512]{1,0:T(8,128)(2,1)}, u32[]{:S(2)}) copy-start(bf16[2048,512]{1,0:T(8,128)(2,1)} %param.18) | copy-start | bytes 6291460
  155.4 8.8 %all-to-all-start.4 = ((f32[4,1,1024]{2,1,0:T(1,128)}), f32[4,1,1024]{2,1,0:T(1,128)S(1)}, u32[]{:S(2)}, u32[]{:S(2)}) async-start(f32[4,1,1024]{2,1,0:T(1,128)} %reshape.715), calls=%async_computation.4 | async-start | bytes 32768 | tf_op jit(solution)/shard_map/all_to_all | solution.py:151
  164.2 8.8 %all-to-all-start.2 = ((f32[4,1,1024]{2,1,0:T(1,128)}), f32[4,1,1024]{2,1,0:T(1,128)S(1)}, u32[]{:S(2)}, u32[]{:S(2)}) async-start(f32[4,1,1024]{2,1,0:T(1,128)} %reshape.713), calls=%async_computation.2 | async-start | bytes 32768 | tf_op jit(solution)/shard_map/all_to_all | solution.py:150
  173.0 6.5 %copy-start.3 = (bf16[512,256]{1,0:T(8,128)(2,1)S(1)}, bf16[512,256]{1,0:T(8,128)(2,1)}, u32[]{:S(2)}) copy-start(bf16[512,256]{1,0:T(8,128)(2,1)} %param.13) | copy-start | bytes 786436
  173.0 6.6 %copy-start.4 = (bf16[512,256]{1,0:T(8,128)(2,1)S(1)}, bf16[512,256]{1,0:T(8,128)(2,1)}, u32[]{:S(2)}) copy-start(bf16[512,256]{1,0:T(8,128)(2,1)} %param.14) | copy-start | bytes 786436
  173.0 0.6 copy-start.5
  173.6 96.9 %all-to-all-start.3 = ((bf16[4,16,64,512]{3,2,1,0:T(8,128)(2,1)}), bf16[4,16,64,512]{3,2,1,0:T(8,128)(2,1)}, u32[]{:S(2)}, u32[]{:S(2)}) async-start(bf16[4,16,64,512]{3,2,1,0:T(8,128)(2,1)} %convert_bitcast_fusion), calls=%async_computation.3 | async-start | bytes 8388608 | tf_op jit(solution)/shard_map/all_to_all | solution.py:147
  182.9 3.5 %copy-start.2 = (bf16[512,2048]{1,0:T(8,128)(2,1)S(1)}, bf16[512,2048]{1,0:T(8,128)(2,1)}, u32[]{:S(2)}) copy-start(bf16[512,2048]{1,0:T(8,128)(2,1)} %all-gather.2.cloned.1.call-done) | copy-start | bytes 6291460
  185.2 3.9 %copy-start.6 = (f32[4,1,1024]{2,1,0:T(1,128)S(1)}, f32[4,1,1024]{2,1,0:T(1,128)}, u32[]{:S(2)}) copy-start(f32[4,1,1024]{2,1,0:T(1,128)} %copy-done.5) | copy-start | bytes 49156
  185.2 6.1 %copy-start.8 = (pred[32]{0:T(512)(128)(4,1)S(1)}, pred[32]{0:T(512)(128)(4,1)}, u32[]{:S(2)}) copy-start(pred[32]{0:T(512)(128)(4,1)} %get-tuple-element.8) | copy-start | bytes 100
  270.5 3.0 %copy-start.7 = (pred[8,4]{1,0:T(8,128)(4,1)S(1)}, pred[8,4]{1,0:T(8,128)(4,1)}, u32[]{:S(2)}) copy-start(pred[8,4]{1,0:T(8,128)(4,1)} %get-tuple-element.10) | copy-start | bytes 100
  273.8 2.2 copy-start.1
Sparse Core Ops, SparseCore 0:
  8.9 25.2 all-gather.1
where the time goes:
time: 284 us; the launch traced here: 283 us
  waiting for transfers between devices  169 us (60%)
  other arithmetic  29.7 us (10%)
  matrix products  26.6 us (9%)
  starting transfers between devices  22.7 us (8%)
  local copies, waits for them, and re-layouts  20.7 us (7%)
  between operations  13.8 us (5%)
    all_to_all x1, waiting for transfers between devices, body(): lax.all_to_all(weighted_here, 'st', split_axis=0, concat_axis=0, tiled=True)  79 us
    all_to_all x1, waiting for transfers between devices, body(): lax.all_to_all(outgoing, 'st', split_axis=0, concat_axis=0, tiled=True)  66.4 us
    all_gather x1, waiting for transfers between devices, body(): shard_cols = lax.all_gather(tokens, 'tp', axis=1, tiled=True)  18.3 us
    select_n x2, other arithmetic, body(): jnp.take(kv_own, indices, axis=0)  14.2 us
    dot_general x1, matrix products, partial_attend(): jnp.einsum('...tgd,...rgd->...gtr', query_block, key_part, preferred_elem...  7.7 us
    gather x1, local copies, waits for them, and re-layouts, body(): jnp.take(kv_own, indices, axis=0)  7.55 us
    all_to_all x1, starting transfers between devices, body(): lax.all_to_all(wanted, 'st', split_axis=0, concat_axis=0, tiled=True)  6.35 us
  transfers between devices with their start and end apart: 6, of which 4 were waited for; matrix products, arithmetic and copies ran while one was open for 22% of the time, Pallas kernels for 0%

commit v1 on v0

--- a/solution.py
+++ b/solution.py
@@ -1,6 +1,10 @@
+import functools
+
 import jax
 import jax.numpy as jnp
 from jax import lax
+from jax.experimental import pallas as pl
+from jax.experimental.pallas import tpu as pltpu
 from jax.sharding import PartitionSpec as P
 
 RET_DIM = 256
@@ -167,6 +171,336 @@
         token_count, groups * (RET_DIM + HEAD_DIM)
     )
 
+MESH = pl.DeviceIdType.MESH
+NONE = -1e30
+CHUNK = 128
+
+
+def mixer_kernel(
+    S, C, NP, PR,
+    tok, wq, wg, keys, vals, bias, out,
+    xg, qbuf, bin_, rin, sin_, rout, sout, gates,
+    xsend, xrecv, bsend, brecv, qsl, qsr, qrecv, rsend, rrecv, ssend, srecv,
+):
+    s = lax.axis_index("st")
+    tp = lax.axis_index("tp")
+    core = lax.rem(tp, 2)
+    sib = tp + 1 - 2 * core
+    opp = lax.rem(tp + 2, 4)
+    diag = lax.rem(sib + 2, 4)
+    CH = qbuf.shape[2]
+    depth = tok.shape[1]
+    scale = HEAD_DIM ** (-0.5)
+
+    barrier = pltpu.get_barrier_semaphore()
+    for peer in (sib, opp):
+        pl.semaphore_signal(barrier, inc=1, device_id={"tp": peer}, device_id_type=MESH)
+    for k in range(1, S):
+        pl.semaphore_signal(
+            barrier, inc=1, device_id={"st": lax.rem(s + k, S)}, device_id_type=MESH
+        )
+    pl.semaphore_wait(barrier, S + 1)
+
+    def rows(i):
+        return pl.ds(pl.multiple_of(i * CH, CH), CH)
+
+    def xcopy(kind, i):
+        src = tok.at[rows(i)] if kind < 2 else xg.at[opp, rows(i)]
+        slot = tp if kind < 2 else opp
+        return pltpu.make_async_remote_copy(
+            src_ref=src, dst_ref=xg.at[slot, rows(i)],
+            send_sem=xsend.at[kind, i], recv_sem=xrecv.at[kind, i],
+            device_id={"tp": opp if kind == 0 else sib}, device_id_type=MESH,
+        )
+
+    def bcopy(k):
+        o = lax.rem(s + k, S)
+        return pltpu.make_async_remote_copy(
+            src_ref=bias.at[o], dst_ref=bin_.at[s],
+            send_sem=bsend.at[k], recv_sem=brecv.at[k],
+            device_id={"st": o}, device_id_type=MESH,
+        )
+
+    for i in range(C):
+        xcopy(0, i).start()
+        xcopy(1, i).start()
+    for k in range(1, S):
+        bcopy(k).start()
+    bin_[s] = bias[s]
+
+    def qcopy(u, i, right):
+        return pltpu.make_async_remote_copy(
+            src_ref=qbuf.at[u, i], dst_ref=qbuf.at[u, i],
+            send_sem=(qsr if right else qsl).at[u, i], recv_sem=qrecv.at[u, i],
+            device_id={"st": s + 1 if right else s - 1}, device_id_type=MESH,
+        )
+
+    def rcopies(u, i, left):
+        if left:
+            slot = u
+            dev = s - 1
+        else:
+            slot = jnp.where(s + 1 == u, S, u)
+            dev = s + 1
+        return (
+            pltpu.make_async_remote_copy(
+                src_ref=rout.at[u, i], dst_ref=rin.at[slot, i],
+                send_sem=rsend.at[u, i], recv_sem=rrecv.at[slot, i],
+                device_id={"st": dev}, device_id_type=MESH,
+            ),
+            pltpu.make_async_remote_copy(
+                src_ref=sout.at[u, i], dst_ref=sin_.at[slot, i],
+                send_sem=ssend.at[u, i], recv_sem=srecv.at[slot, i],
+                device_id={"st": dev}, device_id_type=MESH,
+            ),
+        )
+
+    def recv_result(slot, i):
+        pltpu.make_async_remote_copy(
+            src_ref=rin.at[slot, i], dst_ref=rin.at[slot, i],
+            send_sem=rsend.at[0, i], recv_sem=rrecv.at[slot, i],
+            device_id={"st": lax.rem(s + 1, S)}, device_id_type=MESH,
+        ).wait_recv()
+        pltpu.make_async_remote_copy(
+            src_ref=sin_.at[slot, i], dst_ref=sin_.at[slot, i],
+            send_sem=ssend.at[0, i], recv_sem=srecv.at[slot, i],
+            device_id={"st": lax.rem(s + 1, S)}, device_id_type=MESH,
+        ).wait_recv()
+
+    def project(i):
+        xcopy(0, i).wait_recv()
+        xcopy(2, i).start()
+        acc = jnp.dot(
+            tok[rows(i)], wq[pl.ds(pl.multiple_of(tp * depth, depth), depth)],
+            preferred_element_type=jnp.float32,
+        )
+        gate = lax.dot_general(
+            wg[tp], tok[rows(i)], (((1,), (1,)), ((), ())), preferred_element_type=jnp.float32
+        )
+        xcopy(1, i).wait_recv()
+        for j in (opp, sib, diag):
+            if j is diag:
+                xcopy(2, i).wait_recv()
+            part = xg[j, rows(i)]
+            acc += jnp.dot(
+                part, wq[pl.ds(pl.multiple_of(j * depth, depth), depth)],
+                preferred_element_type=jnp.float32,
+            )
+            gate += lax.dot_general(
+                wg[j], part, (((1,), (1,)), ((), ())), preferred_element_type=jnp.float32
+            )
+        gates[i] = jax.nn.sigmoid(gate[:8])
+        qbuf[s, i] = acc.astype(jnp.bfloat16)
+
+    def attend(u, i):
+        sc = lax.dot_general(
+            keys[...], qbuf[u, i], (((1,), (1,)), ((), ())), preferred_element_type=jnp.float32
+        ) * scale
+        sc = sc.reshape(NP, PR, CH) + bin_[u, i][:NP][:, None, :]
+        top = jnp.max(jnp.max(sc, 0), 0, keepdims=True)
+        ex = jnp.exp(sc - top[None])
+        tot = jnp.sum(jnp.sum(ex, 0), 0, keepdims=True)
+        part = jnp.dot(
+            vals[...], ex.reshape(NP * PR, CH).astype(jnp.bfloat16),
+            preferred_element_type=jnp.float32,
+        )
+        rout[u, i] = part.astype(jnp.bfloat16)
+        sout[u, i] = jnp.concatenate(
+            [jnp.broadcast_to(top, (4, CH)), jnp.broadcast_to(tot, (4, CH))], 0
+        )
+
+    def merge(u, i, slot):
+        a, b = sout[u, i], sin_[slot, i]
+        ma, ta, mb, tb = a[0:1], a[4:5], b[0:1], b[4:5]
+        top = jnp.maximum(ma, mb)
+        fa, fb = jnp.exp(ma - top), jnp.exp(mb - top)
+        tot = fa * ta + fb * tb
+        mixed = rout[u, i].astype(jnp.float32) * fa + rin[slot, i].astype(jnp.float32) * fb
+        rout[u, i] = mixed.astype(jnp.bfloat16)
+        sout[u, i] = jnp.concatenate(
+            [jnp.broadcast_to(top, (4, CH)), jnp.broadcast_to(tot, (4, CH))], 0
+        )
+
+    for k in range(1, S):
+        bcopy(k).wait_recv()
+
+    def step(t, carry):
+        def forward(u, c):
+            k = jnp.abs(s - u)
+            i = t - k
+
+            @pl.when((u != s) & (i >= 0) & (i < C))
+            def _():
+                qcopy(u, i, True).wait_recv()
+
+                @pl.when((u < s) & (s < S - 1))
+                def _():
+                    qcopy(u, i, True).start()
+
+                @pl.when((u > s) & (s > 0))
+                def _():
+                    qcopy(u, i, False).start()
+
+            return c
+
+        lax.fori_loop(0, S, forward, 0)
+
+        @pl.when(t < C)
+        def _():
+            project(t)
+
+            @pl.when(s < S - 1)
+            def _():
+                qcopy(s, t, True).start()
+
+            @pl.when(s > 0)
+            def _():
+                qcopy(s, t, False).start()
+
+        def work(u, c):
+            k = jnp.abs(s - u)
+            i = t - k
+
+            @pl.when((i >= 0) & (i < C))
+            def _():
+                attend(u, i)
+
+            return c
+
+        lax.fori_loop(0, S, work, 0)
+
+        def back(u, c):
+            k = jnp.abs(s - u)
+            far = jnp.where(u < s, S - 1 - u, u)
+            i = t - (2 * far - k)
+
+            @pl.when((u != s) & (i >= 0) & (i < C))
+            def _():
+                @pl.when(k < far)
+                def _():
+                    recv_result(u, i)
+                    merge(u, i, u)
+
+                @pl.when(u < s)
+                def _():
+                    for copy in rcopies(u, i, True):
+                        copy.start()
+
+                @pl.when(u > s)
+                def _():
+                    for copy in rcopies(u, i, False):
+                        copy.start()
+
+            return c
+
+        lax.fori_loop(0, S, back, 0)
+
+        last = t - 2 * jnp.maximum(s, S - 1 - s)
+
+        @pl.when((last >= 0) & (last < C))
+        def _():
+            @pl.when(s < S - 1)
+            def _():
+                recv_result(s, last)
+                merge(s, last, s)
+
+            @pl.when(s > 0)
+            def _():
+                recv_result(S, last)
+                merge(s, last, S)
+
+            ratio = gates[last][0:1] / sout[s, last][4:5]
+            res = rout[s, last].astype(jnp.float32) * ratio
+            out[rows(last)] = res.T.astype(jnp.bfloat16)
+
+        return carry
+
+    lax.fori_loop(0, C + 2 * (S - 1), step, 0)
+
+    for i in range(C):
+        for kind in range(3):
+            xcopy(kind, i).wait_send()
+    for k in range(1, S):
+        bcopy(k).wait_send()
+
+    def drain(n, c):
+        u, i = n // C, n % C
+
+        @pl.when((u <= s) & (s < S - 1))
+        def _():
+            qcopy(u, i, True).wait_send()
+
+        @pl.when((u >= s) & (s > 0))
+        def _():
+            qcopy(u, i, False).wait_send()
+
+        @pl.when(u < s)
+        def _():
+            for copy in rcopies(u, i, True):
+                copy.wait_send()
+
+        @pl.when(u > s)
+        def _():
+            for copy in rcopies(u, i, False):
+                copy.wait_send()
+
+        return c
+
+    lax.fori_loop(0, S * C, drain, 0)
+
+
+def fast_body(
+    tokens, ret_query, ret_key, ret_value, w_query, w_key, w_value, w_gate, store, passage_ids
+):
+    S = lax.axis_size("st")
+    ntp = lax.axis_size("tp")
+    head = lax.axis_index("tp")
+    T, depth = tokens.shape
+    NP, PR, D = store.shape
+    C = T // CHUNK
+    per = CHUNK // BLOCK
+    NPP = -(-NP // 8) * 8
+    retained = retain(ret_query, ret_key, ret_value, head)
+    flat = store.reshape(NP * PR, D)
+    keys = jnp.dot(flat, w_key, preferred_element_type=jnp.float32).astype(jnp.bfloat16)
+    vals = lax.dot_general(
+        w_value, flat, (((0,), (1,)), ((), ())), preferred_element_type=jnp.float32
+    ).astype(jnp.bfloat16)
+    gate_row = lax.dynamic_slice_in_dim(w_gate, head, 1, 1).reshape(ntp, 1, depth)
+    wg = jnp.broadcast_to(gate_row, (ntp, 16, depth))
+    names = jnp.arange(S * NP, dtype=jnp.int32)
+    counts = jnp.sum((passage_ids[:, :, None] == names).astype(jnp.float32), 1)
+    bias = jnp.where(counts > 0, jnp.log(jnp.maximum(counts, 1.0)), NONE)
+    bias = bias.reshape(C, per, S, NP).transpose(2, 0, 3, 1)
+    bias = jnp.pad(bias, ((0, 0), (0, 0), (0, NPP - NP), (0, 0)), constant_values=NONE)
+    bias = jnp.repeat(bias, BLOCK, axis=3)
+
+    vm = pl.BlockSpec(memory_space=pltpu.VMEM)
+    dma = pltpu.SemaphoreType.DMA
+    retrieved = pl.pallas_call(
+        functools.partial(mixer_kernel, S, C, NP, PR),
+        out_shape=jax.ShapeDtypeStruct((T, HEAD_DIM), jnp.bfloat16),
+        in_specs=[vm] * 6,
+        out_specs=vm,
+        scratch_shapes=[
+            pltpu.VMEM((ntp, T, depth), jnp.bfloat16),
+            pltpu.VMEM((S, C, CHUNK, HEAD_DIM), jnp.bfloat16),
+            pltpu.VMEM((S, C, NPP, CHUNK), jnp.float32),
+            pltpu.VMEM((S + 1, C, HEAD_DIM, CHUNK), jnp.bfloat16),
+            pltpu.VMEM((S + 1, C, 8, CHUNK), jnp.float32),
+            pltpu.VMEM((S, C, HEAD_DIM, CHUNK), jnp.bfloat16),
+            pltpu.VMEM((S, C, 8, CHUNK), jnp.float32),
+            pltpu.VMEM((C, 8, CHUNK), jnp.float32),
+            dma((3, C)), dma((3, C)), dma((S,)), dma((S,)),
+            dma((S, C)), dma((S, C)), dma((S, C)),
+            dma((S, C)), dma((S + 1, C)), dma((S, C)), dma((S + 1, C)),
+        ],
+        compiler_params=pltpu.CompilerParams(
+            collective_id=0, has_side_effects=True, vmem_limit_bytes=60 * 1024 * 1024
+        ),
+    )(tokens, w_query, wg, keys, vals, bias)
+    return jnp.concatenate([retained.reshape(T, RET_DIM), retrieved], -1)
+
 
 def solution(mesh):
     placed = (
@@ -181,6 +515,14 @@
         P("st", None, None),
         P(("grp", "st"), None),
     )
-    return jax.shard_map(
-        body, mesh=mesh, in_specs=placed, out_specs=P(("grp", "st"), "tp"), check_vma=False
-    )
+
+    def run(*args):
+        heads = args[4].shape[1] // HEAD_DIM
+        wide = 2 <= mesh.shape["st"] <= 8 and mesh.shape["tp"] == 4
+        fast = wide and heads == mesh.shape["tp"] and args[7].shape[1] == heads
+        return jax.shard_map(
+            fast_body if fast else body,
+            mesh=mesh, in_specs=placed, out_specs=P(("grp", "st"), "tp"), check_vma=False,
+        )(*args)
+
+    return run

time: 284 us -> 102 us (0.36)
  waiting for transfers between devices: 169 us -> 0 us
  Pallas kernels: 0 us -> 81.1 us
  starting transfers between devices: 22.7 us -> 0 us
  other arithmetic: 29.7 us -> 8.37 us
  local copies, waits for them, and re-layouts: 20.7 us -> 2.65 us
  matrix products: 26.6 us -> 9.51 us
  between operations: 13.8 us -> 0.16 us
    all_to_all x5 -> x0, waiting for transfers between devices: 150 us -> none  [the longest x1 79 us: body(): lax.all_to_all(weighted_here, 'st', split_axis=0, concat_axis=0, tiled=True)]
    pallas_call x0 -> x1, Pallas kernels: none -> 81.1 us  [fast_body(): pl.pallas_call(functools.partial(mixer_kernel, S, C, NP, PR), out_shape=j...]
    all_to_all x5 -> x0, starting transfers between devices: 22.7 us -> none  [the longest x1 6.35 us: body(): lax.all_to_all(wanted, 'st', split_axis=0, concat_axis=0, tiled=True)]
    select_n x8 -> x1, other arithmetic: 19.2 us -> 0.01 us  [fast_body(): bias = jnp.where(counts > 0, jnp.log(jnp.maximum(counts, 1.0)), NONE)]
    all_gather x1 -> x0, waiting for transfers between devices: 18.3 us -> none  [body(): shard_cols = lax.all_gather(tokens, 'tp', axis=1, tiled=True)]
    dot_general x7 -> x2, matrix products: 24.3 us -> 7.15 us  [the longest x1 4.46 us: fast_body(): lax.dot_general(w_value, flat, (((0,), (1,)), ((), ())), preferred_elemen...]
    gather x5 -> x0, local copies, waits for them, and re-layouts: 15.7 us -> none  [the longest x1 7.55 us: body(): jnp.take(kv_own, indices, axis=0)]
    unnamed x27 -> x7, local copies, waits for them, and re-layouts: 3.7 us -> 0.22 us
  transfers between devices with their start and end apart: 6 -> 0, of which waited for: 4 -> 0; matrix products, arithmetic and copies ran while one was open for 22% -> 0% of each run, Pallas kernels for 0% -> 0%
where the time goes in v1:
time: 102 us
  Pallas kernels  81.1 us (80%)
  matrix products  9.51 us (9%)
  other arithmetic  8.37 us (8%)
  local copies, waits for them, and re-layouts  2.65 us (3%)
    pallas_call x1, Pallas kernels, fast_body(): pl.pallas_call(functools.partial(mixer_kernel, S, C, NP, PR), out_shape=j...  81.1 us
    dot_general x1, matrix products, fast_body(): lax.dot_general(w_value, flat, (((0,), (1,)), ((), ())), preferred_elemen...  4.46 us
    dot_general x1, matrix products, fast_body(): jnp.dot(flat, w_key, preferred_element_type=jnp.float32)  2.69 us
    dot_general x1, matrix products, retain(): jnp.einsum('sgij,sjge->sige', weights, value_rows.reshape(layout), prefer...  2.37 us

profile of v1, /device:TPU:0, one launch (start us, length us, event | category | flops | bytes accessed | tf_op | source)
XLA Modules:
  0.0 101.8 jit_solution(18216997305552011488)
XLA Ops:
  0.0 0.0 copy-start
  0.0 0.5 multiply_cosine_fusion
  0.6 1.3 %convert.12 = f32[2,256,1,256]{3,1,0,2:T(8,128)S(1)} convert(bf16[2,256,1,256]{3,1,0,2:T(8,128)(2,1)} %bitcast.30) | non-fusion elementwise | flops 131072 | bytes 786432 | tf_op jit(solution)/shard_map/convert_element_type | solution.py:37
  1.8 1.0 convert.13
  2.8 0.9 fusion.13
  3.8 0.1 exponential_select_fusion
  3.9 2.4 %fusion.21 = (f32[2,256]{1,0:T(2,128)S(1)}, f32[2,256,1,256]{3,1,0,2:T(8,128)}) fusion(bf16[2,256,256]{2,1,0:T(8,128)(2,1)} %bitcast.32, f32[2,256,128]{2,1,0:T(8,128)} %get-tuple-element.9, f32[2,256,128]{2,1,0:T(8,128)} %get-tuple-element.10, bf16[2,256,128]{2,1,0:T(8,128)(2,1)} %get-tuple-element.6, bf16[2,256,128]{2,1,0:T(8,128)(2,1)S(1)} %get-tuple-element.5, ...), kind=kOutput, calls=%fused_computation.36 | convolution fusion | flops 135527936 | bytes 1837056 | tf_op jit(solution)/shard_map/sgij,sjge->sige/dot_general | solution.py:51
  6.3 1.3 %multiply_reduce_fusion = f32[2,256]{1,0:T(2,128)S(1)} fusion(f32[2,256,1,256]{3,1,0,2:T(8,128)} %get-tuple-element.14, f32[2,256]{1,0:T(2,128)S(1)} %broadcast_multiply_fusion), kind=kLoop, calls=%fused_computation.9 | loop fusion | flops 392704 | bytes 528384 | tf_op jit(solution)/shard_map/reduce_sum | solution.py:55
  7.6 1.2 %multiply_convert_fusion = bf16[2,256,1,256]{3,1,0,2:T(8,128)(2,1)S(1)} fusion(f32[2,256,1,256]{3,1,0,2:T(8,128)} %get-tuple-element.14, f32[2,256]{1,0:T(2,128)S(1)} %add_rsqrt_fusion, f32[2,256]{1,0:T(2,128)S(1)} %broadcast_multiply_fusion), kind=kLoop, calls=%fused_computation.8 | loop fusion | flops 393216 | bytes 790528 | tf_op jit(solution)/shard_map/convert_element_type | solution.py:56
  8.8 0.8 dynamic-slice_reduce_fusion
  9.6 0.6 broadcast_in_dim.11.wg
  10.2 0.0 copy-done
  10.2 0.0 copy-start.2
  10.2 4.5 %convolution_convert_fusion.vals = bf16[512,768]{1,0:T(8,128)(2,1)} fusion(bf16[2048,512]{1,0:T(8,128)(2,1)} %param.16, bf16[768,2048]{1,0:T(8,128)(2,1)S(1)} %bitcast.28), kind=kOutput, calls=%fused_computation | convolution fusion | flops 1611005952 | bytes 6029312 | tf_op jit(solution)/shard_map/dot_general | solution.py:466
  14.7 0.0 copy-done.2
  14.7 0.0 copy-start.1
  14.7 2.7 %convolution_convert_fusion.1.keys = bf16[768,512]{1,0:T(8,128)(2,1)} fusion(bf16[768,2048]{1,0:T(8,128)(2,1)S(1)} %bitcast.27, bf16[2048,512]{1,0:T(8,128)(2,1)S(1)} %copy-done.2), kind=kOutput, calls=%fused_computation.1 | convolution fusion | flops 1611005952 | bytes 6029312 | tf_op jit(solution)/shard_map/dot_general | solution.py:465
  17.4 0.0 copy-done.1
  17.4 0.1 convert_reduce_fusion
  17.5 0.1 select_n.24
  17.5 0.2 copy.15
  17.8 0.2 broadcast_in_dim.13
  18.0 0.7 reshape.227.bias
  18.7 81.1 %shard_map.100 = bf16[512,512]{1,0:T(8,128)(2,1)} custom-call(bf16[512,512]{1,0:T(8,128)(2,1)} %tok.1, bf16[2048,512]{1,0:T(8,128)(2,1)} %wq.1, bf16[4,16,512]{2,1,0:T(8,128)(2,1)} %broadcast_in_dim.11.wg, bf16[768,512]{1,0:T(8,128)(2,1)} %convolution_convert_fusion.1.keys, bf16[512,768]{1,0:T(8,128)(2,1)} %convolution_convert_fusion.vals, ...), custom_call_target="tpu_custom_call" | custom-call | tf_op jit(solution)/shard_map/pallas_call | solution.py:480
  99.9 2.0 %pad_maximum_fusion = bf16[512,768]{1,0:T(8,128)(2,1)} fusion(bf16[512,512]{1,0:T(8,128)(2,1)} %shard_map.100, bf16[512,256]{1,0:T(8,128)(2,1)S(1)} %bitcast.29), kind=kLoop, calls=%fused_computation.5 | loop fusion | flops 1572864 | bytes 1572864 | tf_op jit(solution)/shard_map/concatenate | solution.py:502
  (7 shorter events, 0.1 us)
Async XLA Ops:
  0.0 10.2 %copy-start = (bf16[6,128,2048]{2,1,0:T(8,128)(2,1)S(1)}, bf16[6,128,2048]{2,1,0:T(8,128)(2,1)}, u32[]{:S(2)}) copy-start(bf16[6,128,2048]{2,1,0:T(8,128)(2,1)} %param.18) | copy-start | bytes 9437188
  10.2 4.5 %copy-start.2 = (bf16[2048,512]{1,0:T(8,128)(2,1)S(1)}, bf16[2048,512]{1,0:T(8,128)(2,1)}, u32[]{:S(2)}) copy-start(bf16[2048,512]{1,0:T(8,128)(2,1)} %param.15) | copy-start | bytes 6291460
  14.7 2.7 %copy-start.1 = (s32[8,4]{0,1:T(4,128)S(1)}, s32[8,4]{0,1:T(4,128)}, u32[]{:S(2)}) copy-start(s32[8,4]{0,1:T(4,128)} %param.19) | copy-start | bytes 388

commit v2 on v1

--- a/solution.py
+++ b/solution.py
@@ -174,11 +174,13 @@
 MESH = pl.DeviceIdType.MESH
 NONE = -1e30
 CHUNK = 128
+LAG = 0
 
 
 def mixer_kernel(
     S, C, NP, PR,
-    tok, wq, wg, keys, vals, bias, out,
+    tok_h, wq_h, wk_h, wv_h, store_h, rq_h, rk_h, rv_h, wg, bias, cosines, sines, decay, out,
+    tok, wq, wk, wv, store, rq, rk, rv, keys, vals, lsem,
     xg, qbuf, bin_, rin, sin_, rout, sout, gates,
     xsend, xrecv, bsend, brecv, qsl, qsr, qrecv, rsend, rrecv, ssend, srecv,
 ):
@@ -191,6 +193,15 @@
     CH = qbuf.shape[2]
     depth = tok.shape[1]
     scale = HEAD_DIM ** (-0.5)
+    loads = [
+        pltpu.make_async_copy(a, b, lsem.at[n])
+        for n, (a, b) in enumerate((
+            (tok_h, tok), (store_h, store), (wk_h, wk), (wq_h, wq), (wv_h, wv),
+            (rq_h, rq), (rk_h, rk), (rv_h, rv),
+        ))
+    ]
+    for load in loads:
+        load.start()
 
     barrier = pltpu.get_barrier_semaphore()
     for peer in (sib, opp):
@@ -200,6 +211,7 @@
             barrier, inc=1, device_id={"st": lax.rem(s + k, S)}, device_id_type=MESH
         )
     pl.semaphore_wait(barrier, S + 1)
+    loads[0].wait()
 
     def rows(i):
         return pl.ds(pl.multiple_of(i * CH, CH), CH)
@@ -267,6 +279,49 @@
             device_id={"st": lax.rem(s + 1, S)}, device_id_type=MESH,
         ).wait_recv()
 
+    def gate_part(j, part):
+        cols = pl.ds(pl.multiple_of(j * depth, depth), depth)
+        return lax.dot_general(
+            wg[:, cols], part, (((1,), (1,)), ((), ())), preferred_element_type=jnp.float32
+        )
+
+    RB = 2 * PR if NP % 2 == 0 else PR
+
+    def key_rows(n, c):
+        r = pl.ds(pl.multiple_of(n * RB, RB), RB)
+        keys[r] = jnp.dot(
+            store[r], wk[...], preferred_element_type=jnp.float32
+        ).astype(jnp.bfloat16)
+        return c
+
+    def value_rows(n, c):
+        r = pl.ds(pl.multiple_of(n * RB, RB), RB)
+        vals[:, r] = jnp.dot(
+            store[r], wv[...], preferred_element_type=jnp.float32
+        ).T.astype(jnp.bfloat16)
+        return c
+
+    def turned(ref, r, factor):
+        half = RET_DIM // 2
+        a = ref[r, :half].astype(jnp.float32)
+        b = ref[r, half:].astype(jnp.float32)
+        cs, sn = cosines[...], sines[...]
+        both = jnp.concatenate([a * cs - b * sn, a * sn + b * cs], -1) * factor
+        return both.astype(jnp.bfloat16)
+
+    def retention(n):
+        r = pl.ds(pl.multiple_of(n * SEQ_LEN, SEQ_LEN), SEQ_LEN)
+        sc = lax.dot_general(
+            turned(rq, r, 1.0), turned(rk, r, RET_DIM ** (-0.5)),
+            (((1,), (1,)), ((), ())), preferred_element_type=jnp.float32,
+        )
+        raw = jnp.dot(
+            (sc * decay[...]).astype(jnp.bfloat16), rv[r], preferred_element_type=jnp.float32
+        )
+        mid = raw - jnp.mean(raw, -1, keepdims=True)
+        var = jnp.mean(mid * mid, -1, keepdims=True)
+        out[r, :RET_DIM] = (mid * lax.rsqrt(var + NORM_EPS)).astype(jnp.bfloat16)
+
     def project(i):
         xcopy(0, i).wait_recv()
         xcopy(2, i).start()
@@ -274,9 +329,7 @@
             tok[rows(i)], wq[pl.ds(pl.multiple_of(tp * depth, depth), depth)],
             preferred_element_type=jnp.float32,
         )
-        gate = lax.dot_general(
-            wg[tp], tok[rows(i)], (((1,), (1,)), ((), ())), preferred_element_type=jnp.float32
-        )
+        gate = gate_part(tp, tok[rows(i)])
         xcopy(1, i).wait_recv()
         for j in (opp, sib, diag):
             if j is diag:
@@ -286,9 +339,7 @@
                 part, wq[pl.ds(pl.multiple_of(j * depth, depth), depth)],
                 preferred_element_type=jnp.float32,
             )
-            gate += lax.dot_general(
-                wg[j], part, (((1,), (1,)), ((), ())), preferred_element_type=jnp.float32
-            )
+            gate += gate_part(j, part)
         gates[i] = jax.nn.sigmoid(gate[:8])
         qbuf[s, i] = acc.astype(jnp.bfloat16)
 
@@ -321,11 +372,34 @@
             [jnp.broadcast_to(top, (4, CH)), jnp.broadcast_to(tot, (4, CH))], 0
         )
 
-    for k in range(1, S):
-        bcopy(k).wait_recv()
+    loads[1].wait()
+    loads[2].wait()
+    lax.fori_loop(0, NP * PR // RB, key_rows, 0)
+    loads[3].wait()
+    steps = C + 2 * (S - 1) + LAG
+    seqs = tok.shape[0] // SEQ_LEN
 
     def step(t, carry):
-        def forward(u, c):
+        @pl.when(t < C)
+        def _():
+            project(t)
+
+            @pl.when(s < S - 1)
+            def _():
+                qcopy(s, t, True).start()
+
+            @pl.when(s > 0)
+            def _():
+                qcopy(s, t, False).start()
+
+        @pl.when(t == 0)
+        def _():
+            loads[4].wait()
+            lax.fori_loop(0, NP * PR // RB, value_rows, 0)
+            for k in range(1, S):
+                bcopy(k).wait_recv()
+
+        def source(u, c):
             k = jnp.abs(s - u)
             i = t - k
 
@@ -341,61 +415,48 @@
                 def _():
                     qcopy(u, i, False).start()
 
-            return c
-
-        lax.fori_loop(0, S, forward, 0)
-
-        @pl.when(t < C)
-        def _():
-            project(t)
-
-            @pl.when(s < S - 1)
+            n = i - LAG
+
+            @pl.when((n >= 0) & (n < C))
             def _():
-                qcopy(s, t, True).start()
-
-            @pl.when(s > 0)
-            def _():
-                qcopy(s, t, False).start()
-
-        def work(u, c):
-            k = jnp.abs(s - u)
-            i = t - k
-
-            @pl.when((i >= 0) & (i < C))
-            def _():
-                attend(u, i)
-
-            return c
-
-        lax.fori_loop(0, S, work, 0)
-
-        def back(u, c):
-            k = jnp.abs(s - u)
+                attend(u, n)
+
             far = jnp.where(u < s, S - 1 - u, u)
-            i = t - (2 * far - k)
-
-            @pl.when((u != s) & (i >= 0) & (i < C))
+            m = t - (2 * far - k) - LAG
+
+            @pl.when((u != s) & (m >= 0) & (m < C))
             def _():
                 @pl.when(k < far)
                 def _():
-                    recv_result(u, i)
-                    merge(u, i, u)
+                    recv_result(u, m)
+                    merge(u, m, u)
 
                 @pl.when(u < s)
                 def _():
-                    for copy in rcopies(u, i, True):
+                    for copy in rcopies(u, m, True):
                         copy.start()
 
                 @pl.when(u > s)
                 def _():
-                    for copy in rcopies(u, i, False):
+                    for copy in rcopies(u, m, False):
                         copy.start()
 
             return c
 
-        lax.fori_loop(0, S, back, 0)
-
-        last = t - 2 * jnp.maximum(s, S - 1 - s)
+        lax.fori_loop(0, S, source, 0)
+
+        first = steps - 1 - seqs
+
+        @pl.when(t == first)
+        def _():
+            for load in loads[5:]:
+                load.wait()
+
+        @pl.when((t >= first) & (t < first + seqs))
+        def _():
+            retention(t - first)
+
+        last = t - 2 * jnp.maximum(s, S - 1 - s) - LAG
 
         @pl.when((last >= 0) & (last < C))
         def _():
@@ -409,13 +470,13 @@
                 recv_result(S, last)
                 merge(s, last, S)
 
-            ratio = gates[last][0:1] / sout[s, last][4:5]
+            ratio = gates[last, pl.ds(tp, 1)] / sout[s, last][4:5]
             res = rout[s, last].astype(jnp.float32) * ratio
-            out[rows(last)] = res.T.astype(jnp.bfloat16)
+            out[rows(last), RET_DIM:] = res.T.astype(jnp.bfloat16)
 
         return carry
 
-    lax.fori_loop(0, C + 2 * (S - 1), step, 0)
+    lax.fori_loop(0, steps, step, 0)
 
     for i in range(C):
         for kind in range(3):
@@ -460,14 +521,16 @@
     C = T // CHUNK
     per = CHUNK // BLOCK
     NPP = -(-NP // 8) * 8
-    retained = retain(ret_query, ret_key, ret_value, head)
+    heads = w_gate.shape[1]
     flat = store.reshape(NP * PR, D)
-    keys = jnp.dot(flat, w_key, preferred_element_type=jnp.float32).astype(jnp.bfloat16)
-    vals = lax.dot_general(
-        w_value, flat, (((0,), (1,)), ((), ())), preferred_element_type=jnp.float32
-    ).astype(jnp.bfloat16)
-    gate_row = lax.dynamic_slice_in_dim(w_gate, head, 1, 1).reshape(ntp, 1, depth)
-    wg = jnp.broadcast_to(gate_row, (ntp, 16, depth))
+    wg = jnp.pad(w_gate.T, ((0, -heads % 16), (0, 0)))
+    places = jnp.arange(SEQ_LEN, dtype=jnp.float32)
+    half = RET_DIM // 2
+    inverse = ROTARY_BASE ** (-jnp.arange(half, dtype=jnp.float32) / half)
+    angles = places[:, None] * inverse
+    log_gamma = jnp.log1p(-jnp.exp2(-5.0 - head.astype(jnp.float32)))
+    offsets = places[:, None] - places[None, :]
+    decay = jnp.where(offsets >= 0.0, jnp.exp(log_gamma * jnp.maximum(offsets, 0.0)), 0.0)
     names = jnp.arange(S * NP, dtype=jnp.int32)
     counts = jnp.sum((passage_ids[:, :, None] == names).astype(jnp.float32), 1)
     bias = jnp.where(counts > 0, jnp.log(jnp.maximum(counts, 1.0)), NONE)
@@ -476,13 +539,22 @@
     bias = jnp.repeat(bias, BLOCK, axis=3)
 
     vm = pl.BlockSpec(memory_space=pltpu.VMEM)
+    hbm = pl.BlockSpec(memory_space=pl.ANY)
+    bf = jnp.bfloat16
     dma = pltpu.SemaphoreType.DMA
-    retrieved = pl.pallas_call(
+    return pl.pallas_call(
         functools.partial(mixer_kernel, S, C, NP, PR),
-        out_shape=jax.ShapeDtypeStruct((T, HEAD_DIM), jnp.bfloat16),
-        in_specs=[vm] * 6,
+        out_shape=jax.ShapeDtypeStruct((T, RET_DIM + HEAD_DIM), jnp.bfloat16),
+        in_specs=[hbm] * 8 + [vm] * 5,
         out_specs=vm,
         scratch_shapes=[
+            pltpu.VMEM((T, depth), bf),
+            pltpu.VMEM(w_query.shape, bf), pltpu.VMEM(w_key.shape, bf),
+            pltpu.VMEM(w_value.shape, bf), pltpu.VMEM(flat.shape, bf),
+            pltpu.VMEM((T, RET_DIM), bf), pltpu.VMEM((T, RET_DIM), bf),
+            pltpu.VMEM((T, RET_DIM), bf),
+            pltpu.VMEM((NP * PR, HEAD_DIM), bf), pltpu.VMEM((HEAD_DIM, NP * PR), bf),
+            dma((8,)),
             pltpu.VMEM((ntp, T, depth), jnp.bfloat16),
             pltpu.VMEM((S, C, CHUNK, HEAD_DIM), jnp.bfloat16),
             pltpu.VMEM((S, C, NPP, CHUNK), jnp.float32),
@@ -498,8 +570,10 @@
         compiler_params=pltpu.CompilerParams(
             collective_id=0, has_side_effects=True, vmem_limit_bytes=60 * 1024 * 1024
         ),
-    )(tokens, w_query, wg, keys, vals, bias)
-    return jnp.concatenate([retained.reshape(T, RET_DIM), retrieved], -1)
+    )(
+        tokens, w_query, w_key, w_value, flat, ret_query, ret_key, ret_value,
+        wg, bias, jnp.cos(angles), jnp.sin(angles), decay,
+    )
 
 
 def solution(mesh):

time: 102 us -> 81.9 us (0.80)
  matrix products: 9.51 us -> 0 us
  Pallas kernels: 81.1 us -> 74.1 us
  other arithmetic: 8.37 us -> 2.8 us
  local copies, waits for them, and re-layouts: 2.65 us -> 4.65 us
    dot_general x3 -> x0, matrix products: 9.51 us -> none  [the longest x1 4.46 us: fast_body(): lax.dot_general(w_value, flat, (((0,), (1,)), ((), ())), preferred_elemen...]
    pallas_call x1, Pallas kernels: 81.1 us -> 74.1 us  [fast_body(): pl.pallas_call(functools.partial(mixer_kernel, S, C, NP, PR), out_shape=j...]
    convert_element_type x4 -> x0, other arithmetic: 3.51 us -> none  [the longest x1 1.27 us: retain(): query_rows.reshape(layout).astype(jnp.float32)]
    concatenate x2 -> x0, other arithmetic: 2.85 us -> none  [the longest x1 1.97 us: fast_body(): return jnp.concatenate([retained.reshape(T, RET_DIM), retrieved], -1)]
    unnamed x7 -> x2, local copies, waits for them, and re-layouts: 0.22 us -> 2.27 us
    pad x0 -> x1, local copies, waits for them, and re-layouts: none -> 1.34 us  [fast_body(): wg = jnp.pad(w_gate.T, ((0, -heads % 16), (0, 0)))]
    reduce_sum x1 -> x0, other arithmetic: 1.29 us -> none  [retain(): jnp.mean(centred * centred, -1, keepdims=True) + NORM_EPS]
    sin x0 -> x1, other arithmetic: none -> 1.22 us  [fast_body(): jnp.sin(angles)]
where the time goes in v2:
time: 81.9 us; the launch traced here: 81.6 us
  Pallas kernels  74.1 us (90%)
  local copies, waits for them, and re-layouts  4.65 us (6%)
  other arithmetic  2.8 us (3%)
    pallas_call x1, Pallas kernels, fast_body(): pl.pallas_call(functools.partial(mixer_kernel, S, C, NP, PR), out_shape=j...  74.1 us
    unnamed x2, local copies, waits for them, and re-layouts  2.27 us

profile of v2, /device:TPU:0, one launch (start us, length us, event | category | flops | bytes accessed | tf_op | source)
XLA Modules:
  0.0 81.6 jit_solution(10638179339809439844)
XLA Ops:
  0.1 0.8 convert_reduce_fusion
  0.9 0.1 select_n.13
  1.0 0.2 copy.15
  1.2 0.2 broadcast_in_dim.8
  1.4 0.7 reshape.23.bias
  2.1 1.3 %pad.8.wg = bf16[16,2048]{1,0:T(8,128)(2,1)} pad(bf16[4,2048]{1,0:T(4,128)(2,1)} %bitcast.5, bf16[]{:T(256)} %constant.9.clone.1), padding=0_12x0_0 | pad | bytes 81922 | tf_op jit(solution)/shard_map/jit(_pad)/pad | solution.py:526
  3.5 0.8 exponential_select_fusion.decay
  4.3 1.2 %fusion.1 = (f32[256,128]{1,0:T(8,128)}, f32[256,128]{1,0:T(8,128)}) fusion(f32[128]{0:T(128)S(1)} %multiply_power_fusion), kind=kLoop, calls=%fused_computation.4 | loop fusion | flops 32768 | bytes 262656 | tf_op jit(solution)/shard_map/sin | solution.py:575
  5.5 74.1 %shard_map.100 = bf16[512,768]{1,0:T(8,128)(2,1)} custom-call(bf16[512,512]{1,0:T(8,128)(2,1)} %tok_h.1, bf16[2048,512]{1,0:T(8,128)(2,1)} %wq_h.1, bf16[2048,512]{1,0:T(8,128)(2,1)} %wk_h.1, bf16[2048,512]{1,0:T(8,128)(2,1)} %wv_h.1, bf16[768,2048]{1,0:T(8,128)(2,1)} %bitcast.3, bf16[512,256]{1,0:T(8,128)(2,1)} %rq_h.1, bf16[512,256]{1,0:T(8,128)(2,1)} %rk_h.1, ...), custom_call_target="tpu_custom_call" | custom-call | tf_op jit(solution)/shard_map/pallas_call | solution.py:545
  79.6 2.1 %copy.17 = bf16[512,768]{1,0:T(8,128)(2,1)} copy(bf16[512,768]{1,0:T(8,128)(2,1)} %shard_map.100) | data formatting | bytes 1572864
  (3 shorter events, 0.0 us)

commit v3 on v2

--- a/solution.py
+++ b/solution.py
@@ -5,6 +5,7 @@
 from jax import lax
 from jax.experimental import pallas as pl
 from jax.experimental.pallas import tpu as pltpu
+import numpy as np
 from jax.sharding import PartitionSpec as P
 
 RET_DIM = 256
@@ -175,11 +176,13 @@
 NONE = -1e30
 CHUNK = 128
 LAG = 0
+HOP = 1
+HALF = HEAD_DIM // 2
 
 
 def mixer_kernel(
     S, C, NP, PR,
-    tok_h, wq_h, wk_h, wv_h, store_h, rq_h, rk_h, rv_h, wg, bias, cosines, sines, decay, out,
+    tok_h, wq_h, wk_h, wv_h, store_h, rq_h, rk_h, rv_h, wg, bias, cosines, sines, out,
     tok, wq, wk, wv, store, rq, rk, rv, keys, vals, lsem,
     xg, qbuf, bin_, rin, sin_, rout, sout, gates,
     xsend, xrecv, bsend, brecv, qsl, qsr, qrecv, rsend, rrecv, ssend, srecv,
@@ -190,7 +193,7 @@
     sib = tp + 1 - 2 * core
     opp = lax.rem(tp + 2, 4)
     diag = lax.rem(sib + 2, 4)
-    CH = qbuf.shape[2]
+    CH = qbuf.shape[3]
     depth = tok.shape[1]
     scale = HEAD_DIM ** (-0.5)
     loads = [
@@ -240,42 +243,30 @@
         bcopy(k).start()
     bin_[s] = bias[s]
 
-    def qcopy(u, i, right):
+    def qcopy(u, i, right, h):
         return pltpu.make_async_remote_copy(
-            src_ref=qbuf.at[u, i], dst_ref=qbuf.at[u, i],
-            send_sem=(qsr if right else qsl).at[u, i], recv_sem=qrecv.at[u, i],
+            src_ref=qbuf.at[u, i, h], dst_ref=qbuf.at[u, i, h],
+            send_sem=(qsr if right else qsl).at[u, i, h], recv_sem=qrecv.at[u, i, h],
             device_id={"st": s + 1 if right else s - 1}, device_id_type=MESH,
         )
 
-    def rcopies(u, i, left):
-        if left:
-            slot = u
-            dev = s - 1
-        else:
-            slot = jnp.where(s + 1 == u, S, u)
-            dev = s + 1
-        return (
-            pltpu.make_async_remote_copy(
-                src_ref=rout.at[u, i], dst_ref=rin.at[slot, i],
-                send_sem=rsend.at[u, i], recv_sem=rrecv.at[slot, i],
-                device_id={"st": dev}, device_id_type=MESH,
-            ),
-            pltpu.make_async_remote_copy(
-                src_ref=sout.at[u, i], dst_ref=sin_.at[slot, i],
-                send_sem=ssend.at[u, i], recv_sem=srecv.at[slot, i],
-                device_id={"st": dev}, device_id_type=MESH,
-            ),
-        )
-
-    def recv_result(slot, i):
+    def rcopy(u, i, left, n):
+        slot = u if left else jnp.where(s + 1 == u, S, u)
+        at = (i,) if n == 2 else (i, n)
+        src, dst = (sout, sin_) if n == 2 else (rout, rin)
+        out_sem, in_sem = (ssend, srecv) if n == 2 else (rsend, rrecv)
+        return pltpu.make_async_remote_copy(
+            src_ref=src.at[(u,) + at], dst_ref=dst.at[(slot,) + at],
+            send_sem=out_sem.at[(u,) + at], recv_sem=in_sem.at[(slot,) + at],
+            device_id={"st": s - 1 if left else s + 1}, device_id_type=MESH,
+        )
+
+    def arrived(data, slot, i, *h):
+        buf, out_sem, in_sem = (rin, rsend, rrecv) if data else (sin_, ssend, srecv)
+        ref = buf.at[(slot, i) + h]
         pltpu.make_async_remote_copy(
-            src_ref=rin.at[slot, i], dst_ref=rin.at[slot, i],
-            send_sem=rsend.at[0, i], recv_sem=rrecv.at[slot, i],
-            device_id={"st": lax.rem(s + 1, S)}, device_id_type=MESH,
-        ).wait_recv()
-        pltpu.make_async_remote_copy(
-            src_ref=sin_.at[slot, i], dst_ref=sin_.at[slot, i],
-            send_sem=ssend.at[0, i], recv_sem=srecv.at[slot, i],
+            src_ref=ref, dst_ref=ref,
+            send_sem=out_sem.at[(0, i) + h], recv_sem=in_sem.at[(slot, i) + h],
             device_id={"st": lax.rem(s + 1, S)}, device_id_type=MESH,
         ).wait_recv()
 
@@ -315,8 +306,16 @@
             turned(rq, r, 1.0), turned(rk, r, RET_DIM ** (-0.5)),
             (((1,), (1,)), ((), ())), preferred_element_type=jnp.float32,
         )
+        offset = (
+            lax.broadcasted_iota(jnp.int32, sc.shape, 0)
+            - lax.broadcasted_iota(jnp.int32, sc.shape, 1)
+        ).astype(jnp.float32)
+        log_gamma = jnp.float32(0.0)
+        for h in range(4):
+            log_gamma = jnp.where(tp == h, float(np.log1p(-(2.0 ** (-5 - h)))), log_gamma)
+        decay = jnp.where(offset >= 0.0, jnp.exp(log_gamma * jnp.maximum(offset, 0.0)), 0.0)
         raw = jnp.dot(
-            (sc * decay[...]).astype(jnp.bfloat16), rv[r], preferred_element_type=jnp.float32
+            (sc * decay).astype(jnp.bfloat16), rv[r], preferred_element_type=jnp.float32
         )
         mid = raw - jnp.mean(raw, -1, keepdims=True)
         var = jnp.mean(mid * mid, -1, keepdims=True)
@@ -341,11 +340,17 @@
             )
             gate += gate_part(j, part)
         gates[i] = jax.nn.sigmoid(gate[:8])
-        qbuf[s, i] = acc.astype(jnp.bfloat16)
+        mixed = acc.astype(jnp.bfloat16)
+        for h in range(2):
+            qbuf[s, i, h] = mixed[:, h * HALF:(h + 1) * HALF]
 
     def attend(u, i):
-        sc = lax.dot_general(
-            keys[...], qbuf[u, i], (((1,), (1,)), ((), ())), preferred_element_type=jnp.float32
+        sc = sum(
+            lax.dot_general(
+                keys[:, h * HALF:(h + 1) * HALF], qbuf[u, i, h],
+                (((1,), (1,)), ((), ())), preferred_element_type=jnp.float32,
+            )
+            for h in range(2)
         ) * scale
         sc = sc.reshape(NP, PR, CH) + bin_[u, i][:NP][:, None, :]
         top = jnp.max(jnp.max(sc, 0), 0, keepdims=True)
@@ -355,28 +360,37 @@
             vals[...], ex.reshape(NP * PR, CH).astype(jnp.bfloat16),
             preferred_element_type=jnp.float32,
         )
-        rout[u, i] = part.astype(jnp.bfloat16)
+        for h in range(2):
+            rout[u, i, h] = part[h * HALF:(h + 1) * HALF].astype(jnp.bfloat16)
         sout[u, i] = jnp.concatenate(
             [jnp.broadcast_to(top, (4, CH)), jnp.broadcast_to(tot, (4, CH))], 0
         )
 
-    def merge(u, i, slot):
+    def merge(u, i, slot, send):
+        arrived(False, slot, i)
         a, b = sout[u, i], sin_[slot, i]
         ma, ta, mb, tb = a[0:1], a[4:5], b[0:1], b[4:5]
         top = jnp.maximum(ma, mb)
         fa, fb = jnp.exp(ma - top), jnp.exp(mb - top)
         tot = fa * ta + fb * tb
-        mixed = rout[u, i].astype(jnp.float32) * fa + rin[slot, i].astype(jnp.float32) * fb
-        rout[u, i] = mixed.astype(jnp.bfloat16)
         sout[u, i] = jnp.concatenate(
             [jnp.broadcast_to(top, (4, CH)), jnp.broadcast_to(tot, (4, CH))], 0
         )
+        if send:
+            send(2)
+        for h in range(2):
+            arrived(True, slot, i, h)
+            mixed = rout[u, i, h].astype(jnp.float32) * fa
+            mixed += rin[slot, i, h].astype(jnp.float32) * fb
+            rout[u, i, h] = mixed.astype(jnp.bfloat16)
+            if send:
+                send(h)
 
     loads[1].wait()
     loads[2].wait()
     lax.fori_loop(0, NP * PR // RB, key_rows, 0)
     loads[3].wait()
-    steps = C + 2 * (S - 1) + LAG
+    steps = C + 2 * HOP * (S - 1) + LAG
     seqs = tok.shape[0] // SEQ_LEN
 
     def step(t, carry):
@@ -384,13 +398,14 @@
         def _():
             project(t)
 
-            @pl.when(s < S - 1)
-            def _():
-                qcopy(s, t, True).start()
-
-            @pl.when(s > 0)
-            def _():
-                qcopy(s, t, False).start()
+            for h in range(2):
+                @pl.when(s < S - 1)
+                def _():
+                    qcopy(s, t, True, h).start()
+
+                @pl.when(s > 0)
+                def _():
+                    qcopy(s, t, False, h).start()
 
         @pl.when(t == 0)
         def _():
@@ -401,19 +416,20 @@
 
         def source(u, c):
             k = jnp.abs(s - u)
-            i = t - k
+            i = t - HOP * k
 
             @pl.when((u != s) & (i >= 0) & (i < C))
             def _():
-                qcopy(u, i, True).wait_recv()
-
-                @pl.when((u < s) & (s < S - 1))
-                def _():
-                    qcopy(u, i, True).start()
-
-                @pl.when((u > s) & (s > 0))
-                def _():
-                    qcopy(u, i, False).start()
+                for h in range(2):
+                    qcopy(u, i, True, h).wait_recv()
+
+                    @pl.when((u < s) & (s < S - 1))
+                    def _():
+                        qcopy(u, i, True, h).start()
+
+                    @pl.when((u > s) & (s > 0))
+                    def _():
+                        qcopy(u, i, False, h).start()
 
             n = i - LAG
 
@@ -422,24 +438,27 @@
                 attend(u, n)
 
             far = jnp.where(u < s, S - 1 - u, u)
-            m = t - (2 * far - k) - LAG
+            m = t - HOP * (2 * far - k) - LAG
 
             @pl.when((u != s) & (m >= 0) & (m < C))
             def _():
+                def send(n):
+                    @pl.when(u < s)
+                    def _():
+                        rcopy(u, m, True, n).start()
+
+                    @pl.when(u > s)
+                    def _():
+                        rcopy(u, m, False, n).start()
+
                 @pl.when(k < far)
                 def _():
-                    recv_result(u, m)
-                    merge(u, m, u)
-
-                @pl.when(u < s)
+                    merge(u, m, u, send)
+
+                @pl.when(k == far)
                 def _():
-                    for copy in rcopies(u, m, True):
-                        copy.start()
-
-                @pl.when(u > s)
-                def _():
-                    for copy in rcopies(u, m, False):
-                        copy.start()
+                    for n in (2, 0, 1):
+                        send(n)
 
             return c
 
@@ -456,23 +475,23 @@
         def _():
             retention(t - first)
 
-        last = t - 2 * jnp.maximum(s, S - 1 - s) - LAG
+        last = t - 2 * HOP * jnp.maximum(s, S - 1 - s) - LAG
 
         @pl.when((last >= 0) & (last < C))
         def _():
             @pl.when(s < S - 1)
             def _():
-                recv_result(s, last)
-                merge(s, last, s)
+                merge(s, last, s, None)
 
             @pl.when(s > 0)
             def _():
-                recv_result(S, last)
-                merge(s, last, S)
+                merge(s, last, S, None)
 
             ratio = gates[last, pl.ds(tp, 1)] / sout[s, last][4:5]
-            res = rout[s, last].astype(jnp.float32) * ratio
-            out[rows(last), RET_DIM:] = res.T.astype(jnp.bfloat16)
+            for h in range(2):
+                res = rout[s, last, h].astype(jnp.float32) * ratio
+                cols = slice(RET_DIM + h * HALF, RET_DIM + (h + 1) * HALF)
+                out[rows(last), cols] = res.T.astype(jnp.bfloat16)
 
         return carry
 
@@ -489,21 +508,23 @@
 
         @pl.when((u <= s) & (s < S - 1))
         def _():
-            qcopy(u, i, True).wait_send()
+            for h in range(2):
+                qcopy(u, i, True, h).wait_send()
 
         @pl.when((u >= s) & (s > 0))
         def _():
-            qcopy(u, i, False).wait_send()
+            for h in range(2):
+                qcopy(u, i, False, h).wait_send()
 
         @pl.when(u < s)
         def _():
-            for copy in rcopies(u, i, True):
-                copy.wait_send()
+            for n in range(3):
+                rcopy(u, i, True, n).wait_send()
 
         @pl.when(u > s)
         def _():
-            for copy in rcopies(u, i, False):
-                copy.wait_send()
+            for n in range(3):
+                rcopy(u, i, False, n).wait_send()
 
         return c
 
@@ -524,13 +545,9 @@
     heads = w_gate.shape[1]
     flat = store.reshape(NP * PR, D)
     wg = jnp.pad(w_gate.T, ((0, -heads % 16), (0, 0)))
-    places = jnp.arange(SEQ_LEN, dtype=jnp.float32)
     half = RET_DIM // 2
-    inverse = ROTARY_BASE ** (-jnp.arange(half, dtype=jnp.float32) / half)
-    angles = places[:, None] * inverse
-    log_gamma = jnp.log1p(-jnp.exp2(-5.0 - head.astype(jnp.float32)))
-    offsets = places[:, None] - places[None, :]
-    decay = jnp.where(offsets >= 0.0, jnp.exp(log_gamma * jnp.maximum(offsets, 0.0)), 0.0)
+    inverse = ROTARY_BASE ** (-np.arange(half, dtype=np.float32) / half)
+    angles = np.arange(SEQ_LEN, dtype=np.float32)[:, None] * inverse.astype(np.float32)
     names = jnp.arange(S * NP, dtype=jnp.int32)
     counts = jnp.sum((passage_ids[:, :, None] == names).astype(jnp.float32), 1)
     bias = jnp.where(counts > 0, jnp.log(jnp.maximum(counts, 1.0)), NONE)
@@ -545,7 +562,7 @@
     return pl.pallas_call(
         functools.partial(mixer_kernel, S, C, NP, PR),
         out_shape=jax.ShapeDtypeStruct((T, RET_DIM + HEAD_DIM), jnp.bfloat16),
-        in_specs=[hbm] * 8 + [vm] * 5,
+        in_specs=[hbm] * 8 + [vm] * 4,
         out_specs=vm,
         scratch_shapes=[
             pltpu.VMEM((T, depth), bf),
@@ -556,23 +573,23 @@
             pltpu.VMEM((NP * PR, HEAD_DIM), bf), pltpu.VMEM((HEAD_DIM, NP * PR), bf),
             dma((8,)),
             pltpu.VMEM((ntp, T, depth), jnp.bfloat16),
-            pltpu.VMEM((S, C, CHUNK, HEAD_DIM), jnp.bfloat16),
+            pltpu.VMEM((S, C, 2, CHUNK, HALF), jnp.bfloat16),
             pltpu.VMEM((S, C, NPP, CHUNK), jnp.float32),
-            pltpu.VMEM((S + 1, C, HEAD_DIM, CHUNK), jnp.bfloat16),
+            pltpu.VMEM((S + 1, C, 2, HALF, CHUNK), jnp.bfloat16),
             pltpu.VMEM((S + 1, C, 8, CHUNK), jnp.float32),
-            pltpu.VMEM((S, C, HEAD_DIM, CHUNK), jnp.bfloat16),
+            pltpu.VMEM((S, C, 2, HALF, CHUNK), jnp.bfloat16),
             pltpu.VMEM((S, C, 8, CHUNK), jnp.float32),
             pltpu.VMEM((C, 8, CHUNK), jnp.float32),
             dma((3, C)), dma((3, C)), dma((S,)), dma((S,)),
-            dma((S, C)), dma((S, C)), dma((S, C)),
-            dma((S, C)), dma((S + 1, C)), dma((S, C)), dma((S + 1, C)),
+            dma((S, C, 2)), dma((S, C, 2)), dma((S, C, 2)),
+            dma((S, C, 2)), dma((S + 1, C, 2)), dma((S, C)), dma((S + 1, C)),
         ],
         compiler_params=pltpu.CompilerParams(
             collective_id=0, has_side_effects=True, vmem_limit_bytes=60 * 1024 * 1024
         ),
     )(
         tokens, w_query, w_key, w_value, flat, ret_query, ret_key, ret_value,
-        wg, bias, jnp.cos(angles), jnp.sin(angles), decay,
+        wg, bias, jnp.asarray(np.cos(angles), jnp.float32), jnp.asarray(np.sin(angles), jnp.float32),
     )
 
 

time: 81.9 us -> 78.2 us (0.955)
  other arithmetic: 2.8 us -> 0.77 us
  Pallas kernels: 74.1 us -> 72.5 us
    pallas_call x1, Pallas kernels: 74.1 us -> 72.5 us  [fast_body(): pl.pallas_call(functools.partial(mixer_kernel, S, C, NP, PR), out_shape=j...]
    sin x1 -> x0, other arithmetic: 1.22 us -> none  [fast_body(): jnp.sin(angles)]
where the time goes in v3:
time: 78.2 us; the launch traced here: 78 us
  Pallas kernels  72.5 us (93%)
  local copies, waits for them, and re-layouts  4.66 us (6%)
    pallas_call x1, Pallas kernels, fast_body(): pl.pallas_call(functools.partial(mixer_kernel, S, C, NP, PR), out_shape=j...  72.5 us
    unnamed x2, local copies, waits for them, and re-layouts  2.27 us

profile of v3, /device:TPU:0, one launch (start us, length us, event | category | flops | bytes accessed | tf_op | source)
XLA Modules:
  0.0 78.0 jit_solution(7975082012799306981)
XLA Ops:
  0.0 0.8 convert_reduce_fusion
  0.8 0.1 select_n.9
  0.8 0.2 copy.17
  1.1 0.2 broadcast_in_dim.10
  1.3 0.7 reshape.17.bias
  2.0 1.4 %pad.8.wg = bf16[16,2048]{1,0:T(8,128)(2,1)} pad(bf16[4,2048]{1,0:T(4,128)(2,1)} %bitcast.5, bf16[]{:T(256)} %constant.6.clone.1), padding=0_12x0_0 | pad | bytes 81922 | tf_op jit(solution)/shard_map/jit(_pad)/pad | solution.py:547
  3.4 72.5 %shard_map.118 = bf16[512,768]{1,0:T(8,128)(2,1)} custom-call(bf16[512,512]{1,0:T(8,128)(2,1)} %tok_h.1, bf16[2048,512]{1,0:T(8,128)(2,1)} %wq_h.1, bf16[2048,512]{1,0:T(8,128)(2,1)} %wk_h.1, bf16[2048,512]{1,0:T(8,128)(2,1)} %wv_h.1, bf16[768,2048]{1,0:T(8,128)(2,1)} %bitcast.3, bf16[512,256]{1,0:T(8,128)(2,1)} %rq_h.1, bf16[512,256]{1,0:T(8,128)(2,1)} %rk_h.1, ...), custom_call_target="tpu_custom_call" | custom-call | tf_op jit(solution)/shard_map/pallas_call | solution.py:562
  75.9 2.1 %copy.19 = bf16[512,768]{1,0:T(8,128)(2,1)} copy(bf16[512,768]{1,0:T(8,128)(2,1)} %shard_map.118) | data formatting | bytes 1572864
  (2 shorter events, 0.0 us)
